TPU v7x, 128 devices: a whole 4x4x4 slice. The times are simulated.
128 devices in a mesh: ep: 16 (over z, x), tp: 8 (over y, core).
Axes of the slice: x: 4, y: 4, z: 4, core: 2. Of those that a mesh axis runs over, the one named last changes fastest.
Arguments:
- residual: bfloat16 [2048, 2048], P('ep', 'tp'), may hold values from -61 to 61
- in_gain: float32 [2048], replicated, may hold values from 0.1 to 1.9
- in_weight: bfloat16 [2048, 1024], P(None, 'tp'), may hold values from -0.125 to 0.125
- state: float32 [2, 2048, 4096], P(None, 'ep', 'tp'), may hold values from -3 to 3
- decay_rate: float32 [64, 64], P('tp'), may hold values from 0.1 to 1
- frequency: float32 [64, 64], P('tp'), may hold values from 0 to 200
- log_step: float32 [64], P('tp'), may hold values from -3 to -0.7
- in_coef: float32 [2, 64, 64, 16], P(None, 'tp'), may hold values from -1 to 1
- out_coef: float32 [2, 64, 16, 64], P(None, 'tp'), may hold values from -0.75 to 0.75
- skip_gain: float32 [1024], P('tp'), may hold values from -3 to 3
- out_weight: bfloat16 [1024, 2048], replicated, may hold values from -0.1875 to 0.1875
- mid_gain: float32 [2048], replicated, may hold values from 0.1 to 1.9
- gate_vector: bfloat16 [2048], replicated, may hold values from -0.125 to 0.125
- routes: int32 [2048, 4], P('ep'), may hold values from 0 to 127, all different within a row; in each aligned block of 128 rows (0 to 127, 128 to 255, ...) at most 8 rows name the same one
- route_weight: float32 [2048, 4], P('ep'), may hold values from 0.1 to 1
- expert_gate: bfloat16 [128, 2048, 512], P(('ep', 'tp')), may hold values from -0.125 to 0.125
- expert_up: bfloat16 [128, 2048, 512], P(('ep', 'tp')), may hold values from -0.125 to 0.125
- expert_down: bfloat16 [128, 512, 2048], P(('ep', 'tp')), may hold values from -0.25 to 0.25
- shared_gate: bfloat16 [2048, 4096], P(None, 'ep'), may hold values from -0.125 to 0.125
- shared_up: bfloat16 [2048, 4096], P(None, 'ep'), may hold values from -0.125 to 0.125
- shared_down: bfloat16 [4096, 2048], P('ep'), may hold values from -0.09375 to 0.09375
Outputs:
- layer_out: bfloat16 [2048, 2048], P(('ep', 'tp'))
- new_state: float32 [2, 2048, 4096], P(None, 'ep', 'tp')
Inputs may be any that keep to these rules, and one draw needn't show every extreme that they name: `routes`: each row names 4 different experts. Among the rows of one index of ep no expert is named more than 8 times, a bound that some block reaches.
All inputs are finite; a program needn't handle non-finite values.
Results may differ from a plain program's by a relative error of at most 0.0085.
Values may be sent and summed in bfloat16 or wider, within the bound.
No kernel may reach another device: no remote copies, remote signals or barrier semaphores. Data moves between devices by JAX's collectives and lax.ppermute only.
A program may use at most 128 MiB of HBM per device.

v0:
```python
import jax
import jax.numpy as jnp
from jax import lax
from jax.sharding import PartitionSpec as P

norm_eps = 1e-05
routed_scale = 2.5


def laid_out(blocks, dim):
    dims = list(blocks.shape[1:])
    dims[dim] *= blocks.shape[0]
    return jnp.moveaxis(blocks, 0, dim).reshape(dims)


def from_everyone(array, axis):
    length = lax.axis_size(axis)
    return lax.all_to_all(
        jnp.broadcast_to(array[None], (length, *array.shape)), axis, 0, 0, tiled=True
    )


def gather_directly(array, axis, dim):
    return laid_out(from_everyone(array, axis), dim)


def in_one_piece(arrays, axis, split_dim, concat_dim, along):
    both = jnp.concatenate(arrays, axis=along)
    result, at, finished = (
        lax.all_to_all(both, axis, split_axis=split_dim, concat_axis=concat_dim, tiled=True),
        0,
        [],
    )
    for a in arrays:
        finished.append(lax.slice_in_dim(result, at, at + a.shape[along], axis=along))
        at += a.shape[along]
    return tuple(finished)


def in_blocks(array, dim, length):
    before, after = (array.shape[:dim], array.shape[dim + 1 :])
    return jnp.moveaxis(array.reshape(*before, length, -1, *after), dim, 0)


def sent_and_summed(array, axis, dim):
    length = lax.axis_size(axis)
    blocks = lax.all_to_all(in_blocks(array, dim, length), axis, 0, 0, tiled=True)
    return jnp.sum(blocks.astype(jnp.float32), axis=0)


def layer_norm(values, gain_vec):
    row_mean = jnp.mean(values, axis=-1, keepdims=True)
    row_square = jnp.mean(values * values, axis=-1, keepdims=True)
    return (values - row_mean) * lax.rsqrt(row_square - row_mean * row_mean + norm_eps) * gain_vec


def coefficients(decay_rate, frequency, log_step, in_coef):
    time_step = jnp.exp(log_step)[:, None]
    real_rate = -decay_rate
    magnitude = jnp.exp(real_rate * time_step)
    keep_re = magnitude * jnp.cos(frequency * time_step)
    keep_im = magnitude * jnp.sin(frequency * time_step)
    denominator = real_rate * real_rate + frequency * frequency
    factor_re = ((keep_re - 1.0) * real_rate + keep_im * frequency) / denominator
    factor_im = (keep_im * real_rate - (keep_re - 1.0) * frequency) / denominator
    push_re = factor_re[..., None] * in_coef[0] - factor_im[..., None] * in_coef[1]
    push_im = factor_re[..., None] * in_coef[1] + factor_im[..., None] * in_coef[0]
    return (keep_re, keep_im, push_re, push_im)


def mixer_step(
    normed, in_weight, state, decay_rate, frequency, log_step, in_coef, out_coef, skip_gain
):
    row_count = normed.shape[0]
    group_count, state_count = decay_rate.shape
    keep_re, keep_im, push_re, push_im = coefficients(decay_rate, frequency, log_step, in_coef)
    drive = jnp.dot(normed, in_weight, preferred_element_type=jnp.float32).astype(jnp.bfloat16)
    drive_f = drive.astype(jnp.float32).reshape(row_count, group_count, -1)
    input_re = jnp.einsum("tgh,gph->tgp", drive_f, push_re)
    input_im = jnp.einsum("tgh,gph->tgp", drive_f, push_im)
    old_re = state[0].reshape(row_count, group_count, state_count)
    old_im = state[1].reshape(row_count, group_count, state_count)
    new_re = keep_re * old_re - keep_im * old_im + input_re
    new_im = keep_re * old_im + keep_im * old_re + input_im
    read_out = jnp.einsum("ghp,tgp->tgh", out_coef[0], new_re) - jnp.einsum(
        "ghp,tgp->tgh", out_coef[1], new_im
    )
    read_out = read_out.reshape(row_count, -1) + skip_gain * drive_f.reshape(row_count, -1)
    mixed_rows = jax.nn.gelu(read_out, approximate=True).astype(jnp.bfloat16)
    updated = jnp.stack([new_re.reshape(row_count, -1), new_im.reshape(row_count, -1)])
    return (mixed_rows, updated)


def route_slots(routes, experts):
    flat_routes = routes.reshape(-1)
    onehot = (flat_routes[:, None] == jnp.arange(experts, dtype=jnp.int32)[None, :]).astype(
        jnp.int32
    )
    before = jnp.cumsum(onehot, axis=0) - onehot
    return jnp.sum(before * onehot, axis=1).reshape(routes.shape)


def expert_block(row_block, gate_weight, up_weight, down_weight):
    gate_part = jnp.dot(row_block, gate_weight, preferred_element_type=jnp.float32)
    up_part = jnp.dot(row_block, up_weight, preferred_element_type=jnp.float32)
    hidden = (jax.nn.silu(gate_part) * up_part).astype(jnp.bfloat16)
    return jnp.dot(hidden, down_weight, preferred_element_type=jnp.float32).astype(jnp.bfloat16)


def per_device(
    residual,
    in_gain,
    in_weight,
    state,
    decay_rate,
    frequency,
    log_step,
    in_coef,
    out_coef,
    skip_gain,
    out_weight,
    mid_gain,
    gate_vector,
    routes,
    route_weight,
    expert_gate,
    expert_up,
    expert_down,
    shared_gate,
    shared_up,
    shared_down,
):
    tp_count = lax.axis_size("tp")
    ep_count = lax.axis_size("ep")
    tp_place = lax.axis_index("tp")
    seq_rows, feat_part = residual.shape
    width = feat_part * tp_count
    full_resid = gather_directly(residual, "tp", 1)
    normed = layer_norm(full_resid.astype(jnp.float32), in_gain).astype(jnp.bfloat16)
    mixed_part, new_state = mixer_step(
        normed, in_weight, state, decay_rate, frequency, log_step, in_coef, out_coef, skip_gain
    )
    mixed_rows = lax.all_gather(mixed_part, "tp", axis=1, tiled=True)
    after_mix = full_resid.astype(jnp.float32) + jnp.dot(
        mixed_rows, out_weight, preferred_element_type=jnp.float32
    )
    normed_mid = layer_norm(after_mix, mid_gain).astype(jnp.bfloat16)
    per_dev = seq_rows // tp_count
    own_mid = lax.dynamic_slice_in_dim(normed_mid, tp_place * per_dev, per_dev, 0)
    own_after = lax.dynamic_slice_in_dim(after_mix, tp_place * per_dev, per_dev, 0)
    experts = ep_count * tp_count
    top_count = routes.shape[1]
    capacity = max(2, 2 * seq_rows * top_count // experts)
    slot_rank = route_slots(routes, experts)
    dest_tp = routes % tp_count
    dest_ep = routes // tp_count
    is_mine = dest_tp == tp_place
    slot_place = dest_ep * capacity + slot_rank
    slot_total = ep_count * capacity
    matches = (
        slot_place.reshape(-1)[None, :] == jnp.arange(slot_total, dtype=jnp.int32)[:, None]
    ) & is_mine.reshape(-1)[None, :]
    token_ids = jnp.repeat(jnp.arange(seq_rows, dtype=jnp.int32), top_count)
    slot_token = jnp.sum(jnp.where(matches, token_ids[None, :], 0), axis=1)
    outgoing = normed_mid[slot_token].reshape(ep_count, capacity, width)
    copies = jnp.broadcast_to(own_mid[None], (ep_count, per_dev, width))
    got_slots, got_rows = in_one_piece((outgoing, copies), "ep", 0, 0, 1)
    flat_rows = got_slots.reshape(-1, width)
    result = expert_block(flat_rows, expert_gate[0], expert_up[0], expert_down[0])
    computed = result.reshape(got_slots.shape)
    returned = lax.all_to_all(computed, "ep", split_axis=0, concat_axis=0, tiled=True)
    piece = got_rows.reshape(-1, width)
    gate_part = jnp.dot(piece, shared_gate, preferred_element_type=jnp.float32)
    up_part = jnp.dot(piece, shared_up, preferred_element_type=jnp.float32)
    shared_hidden = (jax.nn.silu(gate_part) * up_part).astype(jnp.bfloat16)
    partial_rows = jnp.dot(shared_hidden, shared_down, preferred_element_type=jnp.float32)
    partial_back = lax.all_to_all(
        partial_rows.reshape(ep_count, per_dev, width).astype(jnp.bfloat16),
        "ep",
        split_axis=0,
        concat_axis=0,
        tiled=True,
    ).astype(jnp.float32)
    shared = jnp.sum(partial_back, axis=0)
    flat_back = returned.reshape(slot_total, width)
    weights = route_weight / jnp.sum(route_weight, axis=-1, keepdims=True) * routed_scale
    picked = flat_back[jnp.where(is_mine, slot_place, 0)].astype(jnp.float32)
    routed_part = jnp.sum(jnp.where(is_mine, weights, 0.0)[..., None] * picked, axis=1)
    routed = sent_and_summed(routed_part.astype(jnp.bfloat16), "tp", 0)
    gate_value = jax.nn.sigmoid(jnp.dot(own_mid, gate_vector, preferred_element_type=jnp.float32))
    layer_out = (own_after + routed + gate_value[:, None] * shared).astype(jnp.bfloat16)
    return (layer_out, new_state)


def solution(mesh):
    return jax.shard_map(
        per_device,
        mesh=mesh,
        in_specs=(
            P("ep", "tp"),
            P(),
            P(None, "tp"),
            P(None, "ep", "tp"),
            P("tp", None),
            P("tp", None),
            P("tp"),
            P(None, "tp", None, None),
            P(None, "tp", None, None),
            P("tp"),
            P(),
            P(),
            P(),
            P("ep", None),
            P("ep", None),
            P(("ep", "tp"), None, None),
            P(("ep", "tp"), None, None),
            P(("ep", "tp"), None, None),
            P(None, "ep"),
            P(None, "ep"),
            P("ep", None),
        ),
        out_specs=(P(("ep", "tp"), None), P(None, "ep", "tp")),
        check_vma=False,
    )
```

profile of v0, /device:TPU:0, one launch (start us, length us, event | category | flops | bytes accessed | tf_op | source)
XLA Modules:
  0.0 138.5 jit_solution(16512454888797237247)
XLA Ops:
  0.7 1.8 %broadcast_in_dim.22 = bf16[8,128,256]{2,1,0:T(8,128)(2,1)} broadcast(bf16[128,256]{1,0:T(8,128)(2,1)} %param.21), dimensions={1,2} | broadcast | bytes 589824 | tf_op jit(solution)/shard_map/broadcast_in_dim | solution.py:19
  2.5 4.6 %all-to-all-start = ((bf16[8,128,256]{2,1,0:T(8,128)(2,1)}), bf16[8,128,256]{2,1,0:T(8,128)(2,1)S(1)}, u32[]{:S(2)}, u32[]{:S(2)}) async-start(bf16[8,128,256]{2,1,0:T(8,128)(2,1)} %broadcast_in_dim.22), calls=%async_computation | async-start | bytes 1048576 | tf_op jit(solution)/shard_map/all_to_all | solution.py:18
  11.6 1.1 fusion.78
  13.3 4.1 %all-to-all-done = bf16[8,128,256]{2,1,0:T(8,128)(2,1)S(1)} async-done(((bf16[8,128,256]{2,1,0:T(8,128)(2,1)}), bf16[8,128,256]{2,1,0:T(8,128)(2,1)S(1)}, u32[]{:S(2)}, u32[]{:S(2)}) %all-to-all-start) | async-done | bytes 524320 | tf_op jit(solution)/shard_map/all_to_all | solution.py:18
  19.9 12.8 %all_gather.3 = bf16[128,1024]{0,1:T(8,128)(2,1)S(1)} all-gather(bf16[128,128]{0,1:T(8,128)(2,1)S(1)} %fusion.50), channel_id=1, replica_groups=mesh['ep'=16,'tp'=8] {'tp'}, dimensions={1}, use_global_device_ids=true | all-gather | bytes 294912 | tf_op jit(solution)/shard_map/all_gather | solution.py:143
  36.1 31.1 %all_to_all.25 = bf16[16,24,2048]{2,1,0:T(8,128)(2,1)S(1)} all-to-all(bf16[16,24,2048]{2,1,0:T(8,128)(2,1)S(1)} %pad_maximum_fusion), channel_id=1, replica_groups=mesh['ep'=16,'tp'=8] {'ep'}, dimensions={0} | all-to-all | bytes 3145728 | tf_op jit(solution)/shard_map/all_to_all | solution.py:30
  67.1 1.2 copy-done.1
  68.8 3.4 %fusion = bf16[16,8,2048]{2,1,0:T(8,128)(2,1)} fusion(bf16[1,512,2048]{2,1,0:T(8,128)(2,1)S(1)} %copy-done, bf16[1,2048,512]{2,1,0:T(8,128)(2,1)} %param.37, bf16[16,24,2048]{2,1,0:T(8,128)(2,1)} %copy-done.1, f32[128,512]{1,0:T(8,128)S(1)} %fusion.4), kind=kOutput, calls=%fused_computation.6 | convolution fusion | flops 537526272 | bytes 5505024 | tf_op jit(solution)/shard_map/dot_general | solution.py:107
  72.2 3.6 %all-to-all-start.2 = ((bf16[16,8,2048]{2,1,0:T(8,128)(2,1)}), bf16[16,8,2048]{2,1,0:T(8,128)(2,1)S(1)}, u32[]{:S(2)}, u32[]{:S(2)}) async-start(bf16[16,8,2048]{2,1,0:T(8,128)(2,1)} %fusion), calls=%async_computation.2 | async-start | bytes 1048576 | tf_op jit(solution)/shard_map/all_to_all | solution.py:171
  76.1 2.3 %slice.48 = bf16[16,16,2048]{2,1,0:T(8,128)(2,1)} slice(bf16[16,24,2048]{2,1,0:T(8,128)(2,1)} %copy-done.1), slice={[0:16], [8:24], [0:2048]} | slice | bytes 2097152 | tf_op jit(solution)/shard_map/slice | solution.py:35
  78.4 8.2 %all-to-all-done.2 = bf16[16,8,2048]{2,1,0:T(8,128)(2,1)S(1)} async-done(((bf16[16,8,2048]{2,1,0:T(8,128)(2,1)}), bf16[16,8,2048]{2,1,0:T(8,128)(2,1)S(1)}, u32[]{:S(2)}, u32[]{:S(2)}) %all-to-all-start.2) | async-done | bytes 524320 | tf_op jit(solution)/shard_map/all_to_all | solution.py:171
  86.6 3.3 %gather_fusion.1 = bf16[512,2048]{1,0:T(8,128)(2,1)} fusion(bf16[128,2048]{1,0:T(8,128)(2,1)S(1)} %bitcast.115, s32[1024]{0:T(1024)S(1)} %pad_clamp_fusion), kind=kCustom, calls=%fused_computation.1 | custom fusion | bytes 4196352 | tf_op jit(solution)/shard_map/gather | solution.py:187
  89.9 4.8 %reshape.146 = f32[128,4,2048]{2,1,0:T(4,128)} reshape(bf16[512,2048]{1,0:T(8,128)(2,1)} %gather_fusion.1) | data formatting | bytes 6291456 | tf_op jit(solution)/shard_map/convert_element_type | solution.py:187
  94.7 6.3 %multiply_reduce_fusion = bf16[128,2048]{1,0:T(8,128)(2,1)} fusion(f32[128,4,2048]{2,1,0:T(4,128)} %reshape.146, f32[128,4]{1,0:T(8,128)S(1)} %copy.87), kind=kLoop, calls=%fused_computation.2 | loop fusion | flops 1835008 | bytes 4720640 | tf_op jit(solution)/shard_map/reduce_sum | solution.py:188
  100.9 4.1 %all-to-all-start.3 = ((bf16[8,16,2048]{2,1,0:T(8,128)(2,1)}), bf16[8,16,2048]{2,1,0:T(8,128)(2,1)}, u32[]{:S(2)}, u32[]{:S(2)}) async-start(bf16[8,16,2048]{2,1,0:T(8,128)(2,1)} %bitcast.126), calls=%async_computation.3 | async-start | bytes 1048576 | tf_op jit(solution)/shard_map/all_to_all | solution.py:47
  105.1 2.4 %fusion.79 = f32[256,256]{1,0:T(8,128)} fusion(bf16[256,2048]{1,0:T(8,128)(2,1)S(1)} %bitcast.118, bf16[2048,256]{1,0:T(8,128)(2,1)} %param.39), kind=kOutput, calls=%fused_computation.129 | convolution fusion | flops 268435456 | bytes 2359296 | tf_op jit(solution)/shard_map/dot_general | solution.py:173
  107.5 3.9 %convolution_convert_fusion = bf16[256,2048]{1,0:T(8,128)(2,1)} fusion(bf16[256,2048]{1,0:T(8,128)(2,1)} %param.41, bf16[256,2048]{1,0:T(8,128)(2,1)S(1)} %bitcast.119, bf16[2048,256]{1,0:T(8,128)(2,1)} %param.40, f32[256,256]{1,0:T(8,128)} %fusion.79), kind=kOutput, calls=%fused_computation.3 | convolution fusion | flops 537788416 | bytes 4456448 | tf_op jit(solution)/shard_map/dot_general | solution.py:176
  111.4 4.0 %all-to-all-done.3 = bf16[8,16,2048]{2,1,0:T(8,128)(2,1)} async-done(((bf16[8,16,2048]{2,1,0:T(8,128)(2,1)}), bf16[8,16,2048]{2,1,0:T(8,128)(2,1)}, u32[]{:S(2)}, u32[]{:S(2)}) %all-to-all-start.3) | async-done | bytes 524320 | tf_op jit(solution)/shard_map/all_to_all | solution.py:47
  115.4 3.7 %all-to-all-start.4 = ((bf16[16,16,2048]{2,1,0:T(8,128)(2,1)}), bf16[16,16,2048]{2,1,0:T(8,128)(2,1)S(1)}, u32[]{:S(2)}, u32[]{:S(2)}) async-start(bf16[16,16,2048]{2,1,0:T(8,128)(2,1)} %bitcast.129), calls=%async_computation.4 | async-start | bytes 2097152 | tf_op jit(solution)/shard_map/all_to_all | solution.py:177
  119.1 1.8 %copy.97 = f32[1,128,512]{2,1,0:T(8,128)} copy(f32[1,128,512]{1,2,0:T(8,128)} %bitcast.125) | data formatting | bytes 524288 | tf_op jit(solution)/shard_map/stack;reshape | solution.py:90
  121.7 1.9 %pad_maximum_fusion.1 = f32[2,128,512]{2,1,0:T(8,128)} fusion(f32[1,128,512]{2,1,0:T(8,128)} %copy.97, f32[1,128,512]{2,1,0:T(8,128)} %copy.96), kind=kLoop, calls=%fused_computation.38 | loop fusion | flops 131072 | bytes 1048576 | tf_op jit(solution)/shard_map/stack | solution.py:90
  123.7 1.1 convert_reduce_fusion.2
  124.9 11.8 %all-to-all-done.4 = bf16[16,16,2048]{2,1,0:T(8,128)(2,1)S(1)} async-done(((bf16[16,16,2048]{2,1,0:T(8,128)(2,1)}), bf16[16,16,2048]{2,1,0:T(8,128)(2,1)S(1)}, u32[]{:S(2)}, u32[]{:S(2)}) %all-to-all-start.4) | async-done | bytes 1048608 | tf_op jit(solution)/shard_map/all_to_all | solution.py:177
  136.8 1.6 %add_convert_fusion = bf16[16,2048]{1,0:T(8,128)(2,1)} fusion(f32[16,2048]{1,0:T(8,128)S(1)} %convert_reduce_fusion, f32[16,2048]{1,0:T(8,128)S(1)} %convert_reduce_fusion.2, f32[128,2048]{1,0:T(8,128)} %copy-done.2, s32[]{:T(128)S(6)} %select_n.41, f32[16]{0:T(128)S(1)} %fusion.18), kind=kLoop, calls=%fused_computation.62 | loop fusion | flops 131072 | bytes 458820 | tf_op jit(solution)/shard_map/convert_element_type | solution.py:191
  (89 shorter events, 12.7 us)
Async XLA Ops:
  0.6 68.1 %copy-start = (bf16[1,512,2048]{2,1,0:T(8,128)(2,1)S(1)}, bf16[1,512,2048]{2,1,0:T(8,128)(2,1)}, u32[]{:S(2)}) copy-start(bf16[1,512,2048]{2,1,0:T(8,128)(2,1)} %param.38) | copy-start | bytes 6291460
  0.6 10.7 %copy-start.10 = (s32[128,4]{0,1:T(4,128)S(1)}, s32[128,4]{0,1:T(4,128)}, u32[]{:S(2)}) copy-start(s32[128,4]{0,1:T(4,128)} %param.34) | copy-start | bytes 6148
  2.5 14.9 %all-to-all-start = ((bf16[8,128,256]{2,1,0:T(8,128)(2,1)}), bf16[8,128,256]{2,1,0:T(8,128)(2,1)S(1)}, u32[]{:S(2)}, u32[]{:S(2)}) async-start(bf16[8,128,256]{2,1,0:T(8,128)(2,1)} %broadcast_in_dim.22), calls=%async_computation | async-start | bytes 1048576 | tf_op jit(solution)/shard_map/all_to_all | solution.py:18
  10.5 2.6 %copy-start.13 = (f32[8,64]{1,0:T(8,128)S(1)}, f32[8,64]{1,0:T(8,128)}, u32[]{:S(2)}) copy-start(f32[8,64]{1,0:T(8,128)} %param.26) | copy-start | bytes 6148
  10.5 2.6 %copy-start.14 = (f32[8,64]{1,0:T(8,128)S(1)}, f32[8,64]{1,0:T(8,128)}, u32[]{:S(2)}) copy-start(f32[8,64]{1,0:T(8,128)} %param.25) | copy-start | bytes 6148
  13.3 4.6 %copy-start.11 = (f32[2048]{0:T(1024)S(1)}, f32[2048]{0:T(1024)}, u32[]{:S(2)}) copy-start(f32[2048]{0:T(1024)} %param.22) | copy-start | bytes 24580
  17.4 1.0 copy-start.7
  17.5 1.4 copy-start.8
  17.6 1.9 %copy-start.9 = (f32[2,8,16,64]{3,2,1,0:T(8,128)S(1)}, f32[2,8,16,64]{3,2,1,0:T(8,128)}, u32[]{:S(2)}) copy-start(f32[2,8,16,64]{3,2,1,0:T(8,128)} %param.29) | copy-start | bytes 196612
  18.4 1.4 copy-start.16
  18.4 14.3 %copy-start.3 = (bf16[1024,2048]{1,0:T(8,128)(2,1)S(1)}, bf16[1024,2048]{1,0:T(8,128)(2,1)}, u32[]{:S(2)}) copy-start(bf16[1024,2048]{1,0:T(8,128)(2,1)} %param.31) | copy-start | bytes 12582916
  19.2 14.4 %copy-start.5 = (f32[128,8,64]{0,2,1:T(8,128)}, f32[128,8,64]{0,2,1:T(8,128)S(1)}, u32[]{:S(2)}) copy-start(f32[128,8,64]{0,2,1:T(8,128)S(1)} %fusion.9) | copy-start | bytes 786436
  32.7 1.9 %copy-start.12 = (f32[2048]{0:T(1024)S(1)}, f32[2048]{0:T(1024)}, u32[]{:S(2)}) copy-start(f32[2048]{0:T(1024)} %param.32) | copy-start | bytes 24580
  33.6 1.0 copy-start.2
  36.0 32.3 %copy-start.6 = (bf16[1,2048,512]{2,1,0:T(8,128)(2,1)S(1)}, bf16[1,2048,512]{2,1,0:T(8,128)(2,1)}, u32[]{:S(2)}) copy-start(bf16[1,2048,512]{2,1,0:T(8,128)(2,1)} %param.36) | copy-start | bytes 6291460
  67.1 1.2 copy-start.1
  72.2 14.4 %all-to-all-start.2 = ((bf16[16,8,2048]{2,1,0:T(8,128)(2,1)}), bf16[16,8,2048]{2,1,0:T(8,128)(2,1)S(1)}, u32[]{:S(2)}, u32[]{:S(2)}) async-start(bf16[16,8,2048]{2,1,0:T(8,128)(2,1)} %fusion), calls=%async_computation.2 | async-start | bytes 1048576 | tf_op jit(solution)/shard_map/all_to_all | solution.py:171
  94.7 10.4 %copy-start.4 = (bf16[16,16,2048]{2,1,0:T(8,128)(2,1)S(1)}, bf16[16,16,2048]{2,1,0:T(8,128)(2,1)}, u32[]{:S(2)}) copy-start(bf16[16,16,2048]{2,1,0:T(8,128)(2,1)} %slice.48) | copy-start | bytes 3145732
  100.9 14.5 %all-to-all-start.3 = ((bf16[8,16,2048]{2,1,0:T(8,128)(2,1)}), bf16[8,16,2048]{2,1,0:T(8,128)(2,1)}, u32[]{:S(2)}, u32[]{:S(2)}) async-start(bf16[8,16,2048]{2,1,0:T(8,128)(2,1)} %bitcast.126), calls=%async_computation.3 | async-start | bytes 1048576 | tf_op jit(solution)/shard_map/all_to_all | solution.py:47
  111.4 7.7 %copy-start.15 = (bf16[2048]{0:T(1024)(128)(2,1)S(1)}, bf16[2048]{0:T(1024)(128)(2,1)}, u32[]{:S(2)}) copy-start(bf16[2048]{0:T(1024)(128)(2,1)} %param.33) | copy-start | bytes 12292
  115.4 21.3 %all-to-all-start.4 = ((bf16[16,16,2048]{2,1,0:T(8,128)(2,1)}), bf16[16,16,2048]{2,1,0:T(8,128)(2,1)S(1)}, u32[]{:S(2)}, u32[]{:S(2)}) async-start(bf16[16,16,2048]{2,1,0:T(8,128)(2,1)} %bitcast.129), calls=%async_computation.4 | async-start | bytes 2097152 | tf_op jit(solution)/shard_map/all_to_all | solution.py:177
where the time goes:
time: 139 us; the launch traced here: 138 us
  blocking collectives  43.9 us (32%)
  waiting for transfers between devices  28.1 us (20%)
  local copies, waits for them, and re-layouts  23 us (17%)
  starting transfers between devices  16 us (12%)
  other arithmetic  14.1 us (10%)
  matrix products  12.4 us (9%)
    all_to_all x1, blocking collectives, in_one_piece(): lax.all_to_all(both, axis, split_axis=split_dim, concat_axis=concat_dim,...  31.1 us
    all_gather x1, blocking collectives, per_device(): mixed_rows = lax.all_gather(mixed_part, 'tp', axis=1, tiled=True)  12.8 us
    all_to_all x1, waiting for transfers between devices, per_device(): lax.all_to_all(partial_rows.reshape(ep_count, per_dev, width).astype(jnp....  11.8 us
    all_to_all x1, waiting for transfers between devices, per_device(): lax.all_to_all(computed, 'ep', split_axis=0, concat_axis=0, tiled=True)  8.19 us
    reduce_sum x1, other arithmetic, per_device(): jnp.sum(jnp.where(is_mine, weights, 0.0)[..., None] * picked, axis=1)  6.28 us
    convert_element_type x1, local copies, waits for them, and re-layouts, per_device(): picked = flat_back[jnp.where(is_mine, slot_place, 0)].astype(jnp.float32)  4.75 us
    all_to_all x1, starting transfers between devices, from_everyone(): lax.all_to_all(jnp.broadcast_to(array[None], (length, *array.shape)), axi...  4.58 us
    all_to_all x1, starting transfers between devices, sent_and_summed(): lax.all_to_all(in_blocks(array, dim, length), axis, 0, 0, tiled=True)  4.14 us
  transfers between devices with their start and end apart: 4, of which 4 were waited for; matrix products, arithmetic and copies ran while one was open for 15% of the time, Pallas kernels for 0%

commit v1 on v0

--- a/solution.py
+++ b/solution.py
@@ -5,6 +5,9 @@
 
 norm_eps = 1e-05
 routed_scale = 2.5
+sources_all_make = lambda buf: jnp.concatenate(
+    lax.all_to_all(jnp.stack([buf] * lax.axis_size("tp"), 0), "tp", 0, 0), 1
+)
 
 
 def laid_out(blocks, dim):
@@ -140,7 +143,7 @@
     mixed_part, new_state = mixer_step(
         normed, in_weight, state, decay_rate, frequency, log_step, in_coef, out_coef, skip_gain
     )
-    mixed_rows = lax.all_gather(mixed_part, "tp", axis=1, tiled=True)
+    mixed_rows = sources_all_make(mixed_part)
     after_mix = full_resid.astype(jnp.float32) + jnp.dot(
         mixed_rows, out_weight, preferred_element_type=jnp.float32
     )

time: 139 us -> 141 us (1.014)
  blocking collectives: 43.9 us -> 30.2 us
  waiting for transfers between devices: 28.1 us -> 35.2 us
  starting transfers between devices: 16 us -> 19.5 us
  local copies, waits for them, and re-layouts: 23 us -> 26.3 us
    all_gather x1 -> x0, blocking collectives: 12.8 us -> none  [per_device(): mixed_rows = lax.all_gather(mixed_part, 'tp', axis=1, tiled=True)]
    all_to_all x0 -> x1, waiting for transfers between devices: none -> 7.41 us  [lax.all_to_all(jnp.stack([buf] * lax.axis_size('tp'), 0), 'tp', 0, 0)]
    all_to_all x0 -> x1, starting transfers between devices: none -> 3.41 us  [lax.all_to_all(jnp.stack([buf] * lax.axis_size('tp'), 0), 'tp', 0, 0)]
    dot_general x1, matrix products: 0.83 us -> 3.03 us  [per_device(): jnp.dot(mixed_rows, out_weight, preferred_element_type=jnp.float32)]
    unnamed x37 -> x45, local copies, waits for them, and re-layouts: 3.58 us -> 5.47 us
  transfers between devices with their start and end apart: 4 -> 5, of which waited for: 4 -> 5; matrix products, arithmetic and copies ran while one was open for 15% -> 15% of each run, Pallas kernels for 0% -> 0%
where the time goes in v1:
time: 141 us; the launch traced here: 140 us
  waiting for transfers between devices  35.2 us (25%)
  blocking collectives  30.2 us (21%)
  local copies, waits for them, and re-layouts  26.3 us (19%)
  starting transfers between devices  19.5 us (14%)
  other arithmetic  14 us (10%)
  matrix products  13.8 us (10%)
    all_to_all x1, blocking collectives, in_one_piece(): lax.all_to_all(both, axis, split_axis=split_dim, concat_axis=concat_dim,...  30.2 us
    all_to_all x1, waiting for transfers between devices, per_device(): lax.all_to_all(partial_rows.reshape(ep_count, per_dev, width).astype(jnp....  11.8 us
    all_to_all x1, waiting for transfers between devices, per_device(): lax.all_to_all(computed, 'ep', split_axis=0, concat_axis=0, tiled=True)  7.67 us
    all_to_all x1, waiting for transfers between devices, lax.all_to_all(jnp.stack([buf] * lax.axis_size('tp'), 0), 'tp', 0, 0)  7.41 us
    reduce_sum x1, other arithmetic, per_device(): jnp.sum(jnp.where(is_mine, weights, 0.0)[..., None] * picked, axis=1)  6.28 us
    unnamed x45, local copies, waits for them, and re-layouts  5.47 us
    all_to_all x1, waiting for transfers between devices, sent_and_summed(): lax.all_to_all(in_blocks(array, dim, length), axis, 0, 0, tiled=True)  4.84 us
    convert_element_type x1, local copies, waits for them, and re-layouts, per_device(): picked = flat_back[jnp.where(is_mine, slot_place, 0)].astype(jnp.float32)  4.73 us
  transfers between devices with their start and end apart: 5, of which 5 were waited for; matrix products, arithmetic and copies ran while one was open for 15% of the time, Pallas kernels for 0%

profile of v1, /device:TPU:0, one launch (start us, length us, event | category | flops | bytes accessed | tf_op | source)
XLA Modules:
  0.0 140.1 jit_solution(12846848356802608968)
XLA Ops:
  0.6 1.8 %broadcast_in_dim.22 = bf16[8,128,256]{2,1,0:T(8,128)(2,1)} broadcast(bf16[128,256]{1,0:T(8,128)(2,1)} %param.21), dimensions={1,2} | broadcast | bytes 589824 | tf_op jit(solution)/shard_map/broadcast_in_dim | solution.py:22
  2.5 4.7 %all-to-all-start = ((bf16[8,128,256]{2,1,0:T(8,128)(2,1)}), bf16[8,128,256]{2,1,0:T(8,128)(2,1)S(1)}, u32[]{:S(2)}, u32[]{:S(2)}) async-start(bf16[8,128,256]{2,1,0:T(8,128)(2,1)} %broadcast_in_dim.22), calls=%async_computation | async-start | bytes 1048576 | tf_op jit(solution)/shard_map/all_to_all | solution.py:21
  14.1 3.4 %all-to-all-done = bf16[8,128,256]{2,1,0:T(8,128)(2,1)S(1)} async-done(((bf16[8,128,256]{2,1,0:T(8,128)(2,1)}), bf16[8,128,256]{2,1,0:T(8,128)(2,1)S(1)}, u32[]{:S(2)}, u32[]{:S(2)}) %all-to-all-start) | async-done | bytes 524320 | tf_op jit(solution)/shard_map/all_to_all | solution.py:21
  22.7 3.4 %all-to-all-start.1 = ((bf16[8,128,128]{1,2,0:T(8,128)(2,1)}), bf16[8,128,128]{1,2,0:T(8,128)(2,1)S(1)}, u32[]{:S(2)}, u32[]{:S(2)}) async-start(bf16[8,128,128]{1,2,0:T(8,128)(2,1)} %stack.4), calls=%async_computation.1 | async-start | bytes 524288 | tf_op jit(solution)/shard_map/all_to_all | solution.py:9
  26.1 7.4 %all-to-all-done.1 = bf16[8,128,128]{1,2,0:T(8,128)(2,1)S(1)} async-done(((bf16[8,128,128]{1,2,0:T(8,128)(2,1)}), bf16[8,128,128]{1,2,0:T(8,128)(2,1)S(1)}, u32[]{:S(2)}, u32[]{:S(2)}) %all-to-all-start.1) | async-done | bytes 262176 | tf_op jit(solution)/shard_map/all_to_all | solution.py:9
  33.5 3.0 %fusion.75 = (f32[128]{0:T(128)S(1)}, f32[128]{0:T(128)S(1)}, f32[128,2048]{1,0:T(8,128)S(1)}) fusion(f32[128,2048]{1,0:T(8,128)S(1)} %bitcast.120, bf16[128,1024]{0,1:T(8,128)(2,1)S(1)} %bitcast.132, bf16[1024,2048]{1,0:T(8,128)(2,1)} %param.31), kind=kOutput, calls=%fused_computation.127 | convolution fusion | flops 537919232 | bytes 6554624 | tf_op jit(solution)/shard_map/dot_general | solution.py:147
  39.0 30.2 %all_to_all.30 = bf16[16,24,2048]{2,1,0:T(8,128)(2,1)S(1)} all-to-all(bf16[16,24,2048]{2,1,0:T(8,128)(2,1)S(1)} %pad_maximum_fusion), channel_id=1, replica_groups=mesh['ep'=16,'tp'=8] {'ep'}, dimensions={0} | all-to-all | bytes 3145728 | tf_op jit(solution)/shard_map/all_to_all | solution.py:33
  69.3 1.2 copy-done.1
  70.9 3.4 %fusion = bf16[16,8,2048]{2,1,0:T(8,128)(2,1)} fusion(bf16[1,512,2048]{2,1,0:T(8,128)(2,1)S(1)} %copy-done, bf16[1,2048,512]{2,1,0:T(8,128)(2,1)} %param.37, bf16[16,24,2048]{2,1,0:T(8,128)(2,1)} %copy-done.1, f32[128,512]{1,0:T(8,128)S(1)} %fusion.4), kind=kOutput, calls=%fused_computation.6 | convolution fusion | flops 537526272 | bytes 5505024 | tf_op jit(solution)/shard_map/dot_general | solution.py:110
  74.3 3.6 %all-to-all-start.3 = ((bf16[16,8,2048]{2,1,0:T(8,128)(2,1)}), bf16[16,8,2048]{2,1,0:T(8,128)(2,1)S(1)}, u32[]{:S(2)}, u32[]{:S(2)}) async-start(bf16[16,8,2048]{2,1,0:T(8,128)(2,1)} %fusion), calls=%async_computation.3 | async-start | bytes 1048576 | tf_op jit(solution)/shard_map/all_to_all | solution.py:174
  78.2 2.3 %slice.48 = bf16[16,16,2048]{2,1,0:T(8,128)(2,1)} slice(bf16[16,24,2048]{2,1,0:T(8,128)(2,1)} %copy-done.1), slice={[0:16], [8:24], [0:2048]} | slice | bytes 2097152 | tf_op jit(solution)/shard_map/slice | solution.py:38
  80.5 7.7 %all-to-all-done.3 = bf16[16,8,2048]{2,1,0:T(8,128)(2,1)S(1)} async-done(((bf16[16,8,2048]{2,1,0:T(8,128)(2,1)}), bf16[16,8,2048]{2,1,0:T(8,128)(2,1)S(1)}, u32[]{:S(2)}, u32[]{:S(2)}) %all-to-all-start.3) | async-done | bytes 524320 | tf_op jit(solution)/shard_map/all_to_all | solution.py:174
  88.2 3.3 %gather_fusion.1 = bf16[512,2048]{1,0:T(8,128)(2,1)} fusion(bf16[128,2048]{1,0:T(8,128)(2,1)S(1)} %bitcast.118, s32[1024]{0:T(1024)S(1)} %pad_clamp_fusion), kind=kCustom, calls=%fused_computation.1 | custom fusion | bytes 4196352 | tf_op jit(solution)/shard_map/gather | solution.py:190
  91.5 4.7 %reshape.156 = f32[128,4,2048]{2,1,0:T(4,128)} reshape(bf16[512,2048]{1,0:T(8,128)(2,1)} %gather_fusion.1) | data formatting | bytes 6291456 | tf_op jit(solution)/shard_map/convert_element_type | solution.py:190
  96.3 6.3 %multiply_reduce_fusion = bf16[128,2048]{1,0:T(8,128)(2,1)} fusion(f32[128,4,2048]{2,1,0:T(4,128)} %reshape.156, f32[128,4]{1,0:T(8,128)S(1)} %copy.88), kind=kLoop, calls=%fused_computation.2 | loop fusion | flops 1835008 | bytes 4720640 | tf_op jit(solution)/shard_map/reduce_sum | solution.py:191
  102.5 4.1 %all-to-all-start.4 = ((bf16[8,16,2048]{2,1,0:T(8,128)(2,1)}), bf16[8,16,2048]{2,1,0:T(8,128)(2,1)}, u32[]{:S(2)}, u32[]{:S(2)}) async-start(bf16[8,16,2048]{2,1,0:T(8,128)(2,1)} %bitcast.129), calls=%async_computation.4 | async-start | bytes 1048576 | tf_op jit(solution)/shard_map/all_to_all | solution.py:50
  106.7 1.7 %fusion.79 = f32[256,256]{1,0:T(8,128)S(1)} fusion(bf16[256,2048]{1,0:T(8,128)(2,1)S(1)} %bitcast.121, bf16[2048,256]{1,0:T(8,128)(2,1)} %param.39), kind=kOutput, calls=%fused_computation.129 | convolution fusion | flops 268435456 | bytes 2359296 | tf_op jit(solution)/shard_map/dot_general | solution.py:176
  108.4 3.8 %convolution_convert_fusion = bf16[256,2048]{1,0:T(8,128)(2,1)} fusion(bf16[256,2048]{1,0:T(8,128)(2,1)} %param.41, bf16[256,2048]{1,0:T(8,128)(2,1)S(1)} %bitcast.122, bf16[2048,256]{1,0:T(8,128)(2,1)} %param.40, f32[256,256]{1,0:T(8,128)S(1)} %fusion.79), kind=kOutput, calls=%fused_computation.3 | convolution fusion | flops 537788416 | bytes 4456448 | tf_op jit(solution)/shard_map/dot_general | solution.py:179
  112.2 4.8 %all-to-all-done.4 = bf16[8,16,2048]{2,1,0:T(8,128)(2,1)} async-done(((bf16[8,16,2048]{2,1,0:T(8,128)(2,1)}), bf16[8,16,2048]{2,1,0:T(8,128)(2,1)}, u32[]{:S(2)}, u32[]{:S(2)}) %all-to-all-start.4) | async-done | bytes 524320 | tf_op jit(solution)/shard_map/all_to_all | solution.py:50
  117.0 3.7 %all-to-all-start.5 = ((bf16[16,16,2048]{2,1,0:T(8,128)(2,1)}), bf16[16,16,2048]{2,1,0:T(8,128)(2,1)S(1)}, u32[]{:S(2)}, u32[]{:S(2)}) async-start(bf16[16,16,2048]{2,1,0:T(8,128)(2,1)} %bitcast.133), calls=%async_computation.5 | async-start | bytes 2097152 | tf_op jit(solution)/shard_map/all_to_all | solution.py:180
  120.7 1.8 %copy.98 = f32[1,128,512]{2,1,0:T(8,128)} copy(f32[1,128,512]{1,2,0:T(8,128)} %bitcast.128) | data formatting | bytes 524288 | tf_op jit(solution)/shard_map/stack;reshape | solution.py:93
  123.3 1.9 %pad_maximum_fusion.1 = f32[2,128,512]{2,1,0:T(8,128)} fusion(f32[1,128,512]{2,1,0:T(8,128)} %copy.98, f32[1,128,512]{2,1,0:T(8,128)} %copy.97), kind=kLoop, calls=%fused_computation.38 | loop fusion | flops 131072 | bytes 1048576 | tf_op jit(solution)/shard_map/stack | solution.py:93
  126.4 11.8 %all-to-all-done.5 = bf16[16,16,2048]{2,1,0:T(8,128)(2,1)S(1)} async-done(((bf16[16,16,2048]{2,1,0:T(8,128)(2,1)}), bf16[16,16,2048]{2,1,0:T(8,128)(2,1)S(1)}, u32[]{:S(2)}, u32[]{:S(2)}) %all-to-all-start.5) | async-done | bytes 1048608 | tf_op jit(solution)/shard_map/all_to_all | solution.py:180
  138.4 1.6 %add_convert_fusion = bf16[16,2048]{1,0:T(8,128)(2,1)} fusion(f32[16,2048]{1,0:T(8,128)S(1)} %convert_reduce_fusion, f32[16,2048]{1,0:T(8,128)S(1)} %convert_reduce_fusion.2, f32[128,2048]{1,0:T(8,128)} %copy-done.2, s32[]{:T(128)S(6)} %select_n.41, f32[16]{0:T(128)S(1)} %fusion.18), kind=kLoop, calls=%fused_computation.62 | loop fusion | flops 131072 | bytes 458820 | tf_op jit(solution)/shard_map/convert_element_type | solution.py:194
  (99 shorter events, 17.4 us)
Async XLA Ops:
  0.6 70.2 %copy-start = (bf16[1,512,2048]{2,1,0:T(8,128)(2,1)S(1)}, bf16[1,512,2048]{2,1,0:T(8,128)(2,1)}, u32[]{:S(2)}) copy-start(bf16[1,512,2048]{2,1,0:T(8,128)(2,1)} %param.38) | copy-start | bytes 6291460
  2.5 10.1 %copy-start.14 = (s32[128,4]{0,1:T(4,128)S(1)}, s32[128,4]{0,1:T(4,128)}, u32[]{:S(2)}) copy-start(s32[128,4]{0,1:T(4,128)} %param.34) | copy-start | bytes 6148
  2.5 15.0 %all-to-all-start = ((bf16[8,128,256]{2,1,0:T(8,128)(2,1)}), bf16[8,128,256]{2,1,0:T(8,128)(2,1)S(1)}, u32[]{:S(2)}, u32[]{:S(2)}) async-start(bf16[8,128,256]{2,1,0:T(8,128)(2,1)} %broadcast_in_dim.22), calls=%async_computation | async-start | bytes 1048576 | tf_op jit(solution)/shard_map/all_to_all | solution.py:21
  10.6 3.3 %copy-start.17 = (f32[8,64]{1,0:T(8,128)S(1)}, f32[8,64]{1,0:T(8,128)}, u32[]{:S(2)}) copy-start(f32[8,64]{1,0:T(8,128)} %param.26) | copy-start | bytes 6148
  10.6 3.3 %copy-start.18 = (f32[8,64]{1,0:T(8,128)S(1)}, f32[8,64]{1,0:T(8,128)}, u32[]{:S(2)}) copy-start(f32[8,64]{1,0:T(8,128)} %param.25) | copy-start | bytes 6148
  14.1 5.6 %copy-start.15 = (f32[2048]{0:T(1024)S(1)}, f32[2048]{0:T(1024)}, u32[]{:S(2)}) copy-start(f32[2048]{0:T(1024)} %param.22) | copy-start | bytes 24580
  18.3 1.4 %copy-start.11 = (bf16[2048,128]{1,0:T(8,128)(2,1)S(1)}, bf16[2048,128]{1,0:T(8,128)(2,1)}, u32[]{:S(2)}) copy-start(bf16[2048,128]{1,0:T(8,128)(2,1)} %param.23) | copy-start | bytes 1572868
  18.4 1.1 copy-start.4
  18.4 1.8 %copy-start.6 = (f32[1,128,512]{1,2,0:T(8,128)S(1)}, f32[1,128,512]{1,2,0:T(8,128)}, u32[]{:S(2)}) copy-start(f32[1,128,512]{1,2,0:T(8,128)} %copy.87) | copy-start | bytes 786436
  18.4 1.8 %copy-start.12 = (f32[2,8,64,16]{2,3,1,0:T(8,128)S(1)}, f32[2,8,64,16]{2,3,1,0:T(8,128)}, u32[]{:S(2)}) copy-start(f32[2,8,64,16]{2,3,1,0:T(8,128)} %param.28) | copy-start | bytes 196612
  19.5 2.0 %copy-start.13 = (f32[2,8,16,64]{3,2,1,0:T(8,128)S(1)}, f32[2,8,16,64]{3,2,1,0:T(8,128)}, u32[]{:S(2)}) copy-start(f32[2,8,16,64]{3,2,1,0:T(8,128)} %param.29) | copy-start | bytes 196612
  19.7 2.1 %copy-start.20 = (f32[128]{0:T(128)S(1)}, f32[128]{0:T(128)}, u32[]{:S(2)}) copy-start(f32[128]{0:T(128)} %param.30) | copy-start | bytes 1540
  20.5 1.2 copy-start.9
  22.7 10.9 %all-to-all-start.1 = ((bf16[8,128,128]{1,2,0:T(8,128)(2,1)}), bf16[8,128,128]{1,2,0:T(8,128)(2,1)S(1)}, u32[]{:S(2)}, u32[]{:S(2)}) async-start(bf16[8,128,128]{1,2,0:T(8,128)(2,1)} %stack.4), calls=%async_computation.1 | async-start | bytes 524288 | tf_op jit(solution)/shard_map/all_to_all | solution.py:9
  33.5 4.0 %copy-start.16 = (f32[2048]{0:T(1024)S(1)}, f32[2048]{0:T(1024)}, u32[]{:S(2)}) copy-start(f32[2048]{0:T(1024)} %param.32) | copy-start | bytes 24580
  36.6 1.0 copy-start.2
  39.0 31.4 %copy-start.10 = (bf16[1,2048,512]{2,1,0:T(8,128)(2,1)S(1)}, bf16[1,2048,512]{2,1,0:T(8,128)(2,1)}, u32[]{:S(2)}) copy-start(bf16[1,2048,512]{2,1,0:T(8,128)(2,1)} %param.36) | copy-start | bytes 6291460
  69.2 1.2 copy-start.1
  74.3 13.9 %all-to-all-start.3 = ((bf16[16,8,2048]{2,1,0:T(8,128)(2,1)}), bf16[16,8,2048]{2,1,0:T(8,128)(2,1)S(1)}, u32[]{:S(2)}, u32[]{:S(2)}) async-start(bf16[16,8,2048]{2,1,0:T(8,128)(2,1)} %fusion), calls=%async_computation.3 | async-start | bytes 1048576 | tf_op jit(solution)/shard_map/all_to_all | solution.py:174
  96.3 10.4 %copy-start.5 = (bf16[16,16,2048]{2,1,0:T(8,128)(2,1)S(1)}, bf16[16,16,2048]{2,1,0:T(8,128)(2,1)}, u32[]{:S(2)}) copy-start(bf16[16,16,2048]{2,1,0:T(8,128)(2,1)} %slice.48) | copy-start | bytes 3145732
  102.5 14.5 %all-to-all-start.4 = ((bf16[8,16,2048]{2,1,0:T(8,128)(2,1)}), bf16[8,16,2048]{2,1,0:T(8,128)(2,1)}, u32[]{:S(2)}, u32[]{:S(2)}) async-start(bf16[8,16,2048]{2,1,0:T(8,128)(2,1)} %bitcast.129), calls=%async_computation.4 | async-start | bytes 1048576 | tf_op jit(solution)/shard_map/all_to_all | solution.py:50
  112.2 8.5 %copy-start.19 = (bf16[2048]{0:T(1024)(128)(2,1)S(1)}, bf16[2048]{0:T(1024)(128)(2,1)}, u32[]{:S(2)}) copy-start(bf16[2048]{0:T(1024)(128)(2,1)} %param.33) | copy-start | bytes 12292
  112.2 10.3 %copy-start.8 = (f32[128,8,64]{0,2,1:T(8,128)S(1)}, f32[128,8,64]{0,2,1:T(8,128)}, u32[]{:S(2)}) copy-start(f32[128,8,64]{0,2,1:T(8,128)} %copy-done.7) | copy-start | bytes 786436
  117.0 21.3 %all-to-all-start.5 = ((bf16[16,16,2048]{2,1,0:T(8,128)(2,1)}), bf16[16,16,2048]{2,1,0:T(8,128)(2,1)S(1)}, u32[]{:S(2)}, u32[]{:S(2)}) async-start(bf16[16,16,2048]{2,1,0:T(8,128)(2,1)} %bitcast.133), calls=%async_computation.5 | async-start | bytes 2097152 | tf_op jit(solution)/shard_map/all_to_all | solution.py:180
  (2 other events, 1.5 us)
